TPU v7x, 32 devices: a whole 2x2x4 slice. The times are simulated.
32 devices in a mesh: grp: 2 (over y), dp: 2 (over x), kv: 4 (over z), tp: 2 (over core).
Axes of the slice: x: 2, y: 2, z: 4, core: 2. Of those that a mesh axis runs over, the one named last changes fastest.
Arguments:
- tokens: bfloat16 [64, 4, 4096], P(('grp', 'dp'), None, 'kv'), parts along dimension 0, may hold values from -6 to 6
- w_query: bfloat16 [4096, 2048], P('kv', 'tp'), may hold values from -0.09375 to 0.09375
- w_forget: bfloat16 [4096, 2048], P('kv', 'tp'), may hold values from -0.09375 to 0.09375
- w_input: bfloat16 [4096, 2048], P('kv', 'tp'), may hold values from -0.09375 to 0.09375
- w_gate: bfloat16 [4096, 2048], P('kv', 'tp'), may hold values from -0.09375 to 0.09375
- w_out: bfloat16 [2048, 4096], P('tp', 'kv'), may hold values from -0.125 to 0.125
- gain: float32 [4096], replicated, may hold values from 0.1 to 1.9
- head_gain: float32 [2048], replicated, may hold values from 0.1 to 1.9
- lower_bound: float32 [2048], replicated, may hold values from 0.05 to 0.9
- state: float32 [64, 16, 128, 128], P(('grp', 'dp', 'kv'), 'tp'), parts along dimension 0, may hold values from -2.4 to 2.4
- last_forget: float32 [64, 4, 2048], P(('grp', 'dp', 'kv'), None, 'tp'), parts along dimension 0, may hold values from 0.3 to 0.99
- last_values: bfloat16 [64, 4, 2048], P(('grp', 'dp', 'kv'), None, 'tp'), parts along dimension 0, may hold values from -6 to 6
- accepted: int32 [64], P(('grp', 'dp', 'kv')), parts along dimension 0, may hold values from 0 to 4
Outputs:
- mixed_out: bfloat16 [64, 4, 4096], P(('grp', 'dp'), None, ('kv', 'tp')), parts along dimension 0
- taken: float32 [64, 16, 128, 128], P(('grp', 'dp', 'kv'), 'tp'), parts along dimension 0
There are 2 independent parts, one for each index of `grp`. A program takes and returns all parts, laid end to end along the dimension named above; an argument that names none is the same for every part. Nothing has to cross between parts.
All inputs are finite; a program needn't handle non-finite values.
Results may differ from a plain program's by a relative error of at most 0.0071.
Values may be sent and summed in bfloat16 or wider, within the bound.
A program may use at most 64 MiB of HBM per device.

v0:
```python
import functools

import jax
import jax.numpy as jnp
from jax import lax
from jax.experimental import pallas as pl
from jax.experimental.pallas import tpu as pltpu
from jax.sharding import PartitionSpec as P

HEAD = 128
EPSILON = 1e-05
CHUNK_HEADS = 4
VMEM_MIB = 56
F32 = jnp.float32
BF16 = jnp.bfloat16


def kernel(
    kv,
    tp,
    tokens,
    w_query,
    w_forget,
    w_input,
    w_gate,
    w_out,
    gain,
    head_gain,
    lower_bound,
    state,
    last_forget,
    last_values,
    accepted,
    tk_v,
    own_v,
    peer_v,
    tok_v,
    gain_v,
    hg_v,
    lb_v,
    lf_v,
    lv_v,
    rows_v,
    scaled_v,
    w_v,
    wo_v,
    st_v,
    tkb_v,
    lfr_v,
    lvr_v,
    ssq_v,
    ssq_r,
    prod_v,
    send_v,
    recv_v,
    gath_v,
    acc_v,
    part_v,
    relay_v,
    load_sem,
    w_sem,
    wo_sem,
    st_sem,
    ssq_ssem,
    ssq_rsem,
    rs_ssem,
    rs_rsem,
    relay_ssem,
    relay_rsem,
    ag_ssem,
    ag_rsem,
    tp_ssem,
    tp_rsem,
):
    me = lax.axis_index("kv")
    tme = lax.axis_index("tp")
    seqs, props, feat = tokens.shape
    own_seqs, heads_dev = state.shape[0], state.shape[1]
    own_rows = own_seqs * props
    rows = seqs * props
    width = gain.shape[1]
    head_cols = heads_dev * HEAD
    chunks = heads_dev // CHUNK_HEADS
    cw = CHUNK_HEADS * HEAD
    half = w_out.shape[1] // tp
    weights = (w_query, w_forget, w_input, w_gate)

    def local(src, dst, sem):
        copy = pltpu.make_async_copy(src, dst, sem)
        copy.start()
        return copy

    tok_c = local(tokens, tok_v, load_sem.at[0])
    gain_c = local(gain, gain_v, load_sem.at[1])

    def load_w(c):
        return [
            local(w.at[:, pl.ds(c * cw, cw)], w_v.at[c, :, pl.ds(i * cw, cw)], w_sem.at[c, i])
            for i, w in enumerate(weights)
        ]

    def load_state(c):
        hs = pl.ds(c * CHUNK_HEADS, CHUNK_HEADS)
        return local(state.at[:, hs], st_v.at[:, hs], st_sem.at[c])

    w_c = [load_w(0)]
    small_c = [
        local(last_forget, lf_v, load_sem.at[2]),
        local(last_values, lv_v, load_sem.at[3]),
        local(head_gain, hg_v, load_sem.at[4]),
        local(lower_bound, lb_v, load_sem.at[5]),
    ]
    st_c = []
    for c in range(chunks):
        st_c.append(load_state(c))
        if c + 1 < chunks:
            w_c.append(load_w(c + 1))
    wo_c = []
    for o in range(tp):
        column = pl.multiple_of(lax.rem(tme + o, tp) * half, half)
        wo_c.append(local(w_out.at[:, pl.ds(column, half)], wo_v.at[o], wo_sem.at[o]))

    barrier = pltpu.get_barrier_semaphore()
    kv_peers = [lax.rem(me + o, kv) for o in range(1, kv)]
    tp_peers = [lax.rem(tme + o, tp) for o in range(1, tp)]
    for peer in kv_peers:
        pl.semaphore_signal(barrier, inc=1, device_id={"kv": peer}, device_id_type=pl.DeviceIdType.MESH)
    for peer in tp_peers:
        pl.semaphore_signal(barrier, inc=1, device_id={"tp": peer}, device_id_type=pl.DeviceIdType.MESH)

    def remote(src, dst, ssem, rsem, axis, peer):
        copy = pltpu.make_async_remote_copy(
            src_ref=src,
            dst_ref=dst,
            send_sem=ssem,
            recv_sem=rsem,
            device_id={axis: peer},
            device_id_type=pl.DeviceIdType.MESH,
        )
        copy.start()
        return copy

    tok_c.wait()
    gain_c.wait()
    for s in range(seqs):
        rows_v[pl.ds(s * props, props), :] = tok_v[s].astype(F32)
    x = rows_v[...]
    my_gain = gain_v[:, pl.ds(pl.multiple_of(me * feat, feat), feat)]
    scaled_v[...] = (x * my_gain).astype(BF16)
    ssq_v[...] = jnp.broadcast_to(jnp.sum(x * x, axis=1, keepdims=True), (rows, HEAD))

    pl.semaphore_wait(barrier, kv - 1 + tp - 1)

    def rows_of(device):
        return pl.ds(pl.multiple_of(device * own_rows, own_rows), own_rows)

    ssq_c = [
        remote(
            ssq_v.at[rows_of(peer)], ssq_r.at[o], ssq_ssem.at[o], ssq_rsem.at[o], "kv", peer
        )
        for o, peer in enumerate(kv_peers)
    ]

    place = lax.broadcasted_iota(jnp.int32, (own_rows, 1), 0)
    prop = lax.rem(place, props)
    seq = place // props

    def old_terms():
        for copy in small_c:
            copy.wait()
        for s in range(own_seqs):
            lfr_v[pl.ds(s * props, props), :] = lf_v[s]
            lvr_v[pl.ds(s * props, props), :] = lv_v[s].astype(F32)
        limit = jnp.zeros((own_rows, 1), jnp.int32)
        for s in range(own_seqs):
            limit = jnp.where(seq == s, accepted[s], limit)
        mask = prop < limit
        old = lfr_v[...]
        decay = jnp.where(mask, old, 1.0)
        weight = jnp.where(mask, 1.0 - old, 0.0)
        after = jnp.ones_like(decay)
        for lag in range(1, props):
            after = after * jnp.where(
                prop < props - lag, pltpu.roll(decay, own_rows - lag, 0), 1.0
            )
        return decay * after, weight * after, lvr_v[...].astype(BF16)

    def take(c, ends, old_weight, old_values):
        st_c[c].wait()
        lane_seq = lax.broadcasted_iota(jnp.int32, (1, own_rows), 1) // props
        for h in range(c * CHUNK_HEADS, (c + 1) * CHUNK_HEADS):
            cols = slice(h * HEAD, (h + 1) * HEAD)
            end_t = ends[:, cols].T
            weight_t = old_weight[:, cols].T
            for s in range(own_seqs):
                mine = jnp.where(lane_seq == s, weight_t, 0.0).astype(BF16)
                added = jnp.dot(mine, old_values[:, cols], preferred_element_type=F32)
                new = end_t[:, s * props : s * props + 1] * st_v[s, h] + added
                tk_v[s, h] = new
                tkb_v[h, pl.ds(s * HEAD, HEAD), :] = new.astype(BF16)

    relayed = kv == 4
    at_end = jnp.logical_or(me == 0, me == kv - 1)
    first = me == 0
    last = me == kv - 1
    if relayed:

        @pl.when(last)
        def _():
            recv_v[:, kv - 2] = jnp.zeros_like(recv_v[:, kv - 2])

        @pl.when(first)
        def _():
            recv_v[:, 0] = jnp.zeros_like(recv_v[:, 0])

    def rs_copy(c, o):
        return pltpu.make_async_remote_copy(
            src_ref=send_v.at[c, rows_of(kv_peers[o])],
            dst_ref=recv_v.at[c, o],
            send_sem=rs_ssem.at[c, o],
            recv_sem=rs_rsem.at[c, o],
            device_id={"kv": kv_peers[o]},
            device_id_type=pl.DeviceIdType.MESH,
        )

    def relay_copy(c, end):
        far, near = (kv - 1, 1) if end == 0 else (0, kv - 2)
        return pltpu.make_async_remote_copy(
            src_ref=send_v.at[c, rows_of(far)],
            dst_ref=relay_v.at[c],
            send_sem=relay_ssem.at[c],
            recv_sem=relay_rsem.at[c],
            device_id={"kv": near},
            device_id_type=pl.DeviceIdType.MESH,
        )

    def send_blocks(c):
        if not relayed:
            for o in range(kv - 1):
                rs_copy(c, o).start()
            return

        @pl.when(first)
        def _():
            relay_copy(c, 0).start()
            rs_copy(c, 1).start()
            if c > 0:
                rs_copy(c - 1, 0).start()
            if c == chunks - 1:
                rs_copy(c, 0).start()

        @pl.when(last)
        def _():
            relay_copy(c, kv - 1).start()
            rs_copy(c, 1).start()
            if c > 0:
                rs_copy(c - 1, 2).start()
            if c == chunks - 1:
                rs_copy(c, 2).start()

        @pl.when(jnp.logical_not(at_end))
        def _():
            rs_copy(c, 0).start()
            rs_copy(c, 2).start()

    def send_on(c):
        if relayed:

            @pl.when(jnp.logical_not(at_end))
            def _():
                relay_copy(c, 0).wait_recv()
                far = rows_of(kv_peers[1])
                send_v[c, far, :] = (prod_v[c, far, :] + relay_v[c].astype(F32)).astype(BF16)
                rs_copy(c, 1).start()

    def wait_blocks(c):
        for o in range(kv - 1):
            if relayed and o == 0:
                pl.when(jnp.logical_not(first))(lambda o=o: rs_copy(c, o).wait_recv())
            elif relayed and o == kv - 2:
                pl.when(jnp.logical_not(last))(lambda o=o: rs_copy(c, o).wait_recv())
            else:
                rs_copy(c, o).wait_recv()

    def wait_sent(c):
        if not relayed:
            for o in range(kv - 1):
                rs_copy(c, o).wait_send()
            return
        rs_copy(c, 1).wait_send()

        @pl.when(first)
        def _():
            relay_copy(c, 0).wait_send()
            rs_copy(c, 0).wait_send()

        @pl.when(last)
        def _():
            relay_copy(c, kv - 1).wait_send()
            rs_copy(c, 2).wait_send()

        @pl.when(jnp.logical_not(at_end))
        def _():
            rs_copy(c, 0).wait_send()
            rs_copy(c, 2).wait_send()

    terms = None
    for c in range(chunks):
        for copy in w_c[c]:
            copy.wait()
        product = jnp.dot(scaled_v[...], w_v[c], preferred_element_type=F32)
        prod_v[c] = product
        send_v[c] = product.astype(BF16)
        send_blocks(c)
        if terms is None:
            terms = old_terms()
        if c > 0:
            send_on(c - 1)
        take(c, *terms)
    send_on(chunks - 1)

    squares = ssq_v[rows_of(me), :]
    for o in range(kv - 1):
        ssq_c[o].wait_recv()
        squares = squares + ssq_r[o]
    row_scale = lax.rsqrt(squares[:, :1] / width + EPSILON)
    mine_rows = rows_of(me)
    ag_c = []

    def recur(c):
        wait_blocks(c)

        def projected(i):
            total = prod_v[c, mine_rows, pl.ds(i * cw, cw)]
            for o in range(kv - 1):
                total = total + recv_v[c, o, :, pl.ds(i * cw, cw)].astype(F32)
            return total * row_scale

        column = pl.multiple_of(tme * head_cols + c * cw, cw)
        floor_gate = lb_v[:, pl.ds(column, cw)]
        forget = floor_gate + (1.0 - floor_gate) * jax.nn.sigmoid(projected(1))
        keys = 1.0 - forget
        queries = jax.nn.silu(projected(0)) * HEAD ** (-0.5)
        values = projected(2)
        gate = jax.nn.silu(projected(3)) * hg_v[:, pl.ds(column, cw)]
        start = forget
        for lag in range(1, props):
            start = start * jnp.where(prop >= lag, pltpu.roll(forget, lag, 0), 1.0)
        reading = queries * start
        results = []
        for h in range(CHUNK_HEADS):
            cols = slice(h * HEAD, (h + 1) * HEAD)
            lhs = jnp.concatenate(
                [jnp.where(seq == s, reading[:, cols], 0.0) for s in range(own_seqs)], axis=1
            ).astype(BF16)
            results.append(
                jnp.dot(lhs, tkb_v[c * CHUNK_HEADS + h], preferred_element_type=F32)
            )
        decay = queries
        for lag in range(props):
            if lag > 0:
                decay = decay * (forget if lag == 1 else pltpu.roll(forget, lag - 1, 0))
            pair = decay * (keys if lag == 0 else pltpu.roll(keys, lag, 0))
            pair = jnp.where(prop >= lag, pair, 0.0)
            moved = values if lag == 0 else pltpu.roll(values, lag, 0)
            for h in range(CHUNK_HEADS):
                cols = slice(h * HEAD, (h + 1) * HEAD)
                score = jnp.sum(pair[:, cols], axis=1, keepdims=True)
                results[h] = results[h] + score * moved[:, cols]
        outs = []
        for h in range(CHUNK_HEADS):
            cols = slice(h * HEAD, (h + 1) * HEAD)
            r = results[h]
            normed = r * lax.rsqrt(jnp.mean(r * r, axis=1, keepdims=True) + EPSILON)
            outs.append((normed * gate[:, cols]).astype(BF16))
        gath_v[c, mine_rows, :] = jnp.concatenate(outs, axis=1)
        ag_c.append(
            [
                remote(
                    gath_v.at[c, mine_rows],
                    gath_v.at[c, mine_rows],
                    ag_ssem.at[c, o],
                    ag_rsem.at[c, o],
                    "kv",
                    peer,
                )
                for o, peer in enumerate(kv_peers)
            ]
        )

    def product_of(c, o):
        term = jnp.dot(
            gath_v[c], wo_v[o, pl.ds(c * cw, cw), :], preferred_element_type=F32
        )
        return term if c == 0 else acc_v[o] + term

    def gathered(c):
        for o in range(kv - 1):
            ag_c[c][o].wait_recv()

    for c in range(chunks):
        recur(c)
    for copy in wo_c:
        copy.wait()
    for c in range(chunks - 1):
        gathered(c)
        for o in range(tp):
            acc_v[o] = product_of(c, o)
    gathered(chunks - 1)
    tp_c = []
    for o in range(1, tp):
        part_v[o - 1] = product_of(chunks - 1, o).astype(BF16)
        tp_c.append(
            remote(
                part_v.at[o - 1],
                peer_v.at[o - 1],
                tp_ssem.at[o - 1],
                tp_rsem.at[o - 1],
                "tp",
                tp_peers[o - 1],
            )
        )
    own_v[...] = product_of(chunks - 1, 0).astype(BF16)
    for copy in tp_c:
        copy.wait_recv()
    for c in range(chunks):
        wait_sent(c)
    for copies in [ssq_c, *ag_c, tp_c]:
        for copy in copies:
            copy.wait_send()


def finish(tk_v, own_v, peer_v, mixed, taken, mix_v, sem):
    tk_c = pltpu.make_async_copy(tk_v, taken, sem.at[0])
    tk_c.start()
    seqs, props, _ = mixed.shape
    total = own_v[...].astype(F32)
    for o in range(peer_v.shape[0]):
        total = total + peer_v[o].astype(F32)
    for s in range(seqs):
        mix_v[s] = total[s * props : (s + 1) * props].astype(BF16)
    mix_c = pltpu.make_async_copy(mix_v, mixed, sem.at[1])
    mix_c.start()
    mix_c.wait()
    tk_c.wait()


def per_device(
    kv,
    tp,
    tokens,
    w_query,
    w_forget,
    w_input,
    w_gate,
    w_out,
    gain,
    head_gain,
    lower_bound,
    state,
    last_forget,
    last_values,
    accepted,
):
    seqs, props, feat = tokens.shape
    own_seqs, heads_dev = state.shape[0], state.shape[1]
    own_rows = own_seqs * props
    rows = seqs * props
    head_cols = heads_dev * HEAD
    chunks = heads_dev // CHUNK_HEADS
    cw = CHUNK_HEADS * HEAD
    half = w_out.shape[1] // tp
    peers = kv - 1
    dma = pltpu.SemaphoreType.DMA
    scratch = [
        pltpu.VMEM(tokens.shape, BF16),
        pltpu.VMEM((1, gain.shape[0]), F32),
        pltpu.VMEM((1, head_gain.shape[0]), F32),
        pltpu.VMEM((1, lower_bound.shape[0]), F32),
        pltpu.VMEM(last_forget.shape, F32),
        pltpu.VMEM(last_values.shape, BF16),
        pltpu.VMEM((rows, feat), F32),
        pltpu.VMEM((rows, feat), BF16),
        pltpu.VMEM((chunks, feat, 4 * cw), BF16),
        pltpu.VMEM((tp, head_cols, half), BF16),
        pltpu.VMEM(state.shape, F32),
        pltpu.VMEM((heads_dev, own_seqs * HEAD, HEAD), BF16),
        pltpu.VMEM((own_rows, head_cols), F32),
        pltpu.VMEM((own_rows, head_cols), F32),
        pltpu.VMEM((rows, HEAD), F32),
        pltpu.VMEM((peers, own_rows, HEAD), F32),
        pltpu.VMEM((chunks, rows, 4 * cw), F32),
        pltpu.VMEM((chunks, rows, 4 * cw), BF16),
        pltpu.VMEM((chunks, peers, own_rows, 4 * cw), BF16),
        pltpu.VMEM((chunks, rows, cw), BF16),
        pltpu.VMEM((tp, rows, half), F32),
        pltpu.VMEM((tp - 1, rows, half), BF16),
        pltpu.VMEM((chunks, own_rows, 4 * cw), BF16),
        dma((6,)),
        dma((chunks, 4)),
        dma((tp,)),
        dma((chunks,)),
        dma((peers,)),
        dma((peers,)),
        dma((chunks, peers)),
        dma((chunks, peers)),
        dma((chunks,)),
        dma((chunks,)),
        dma((chunks, peers)),
        dma((chunks, peers)),
        dma((tp - 1,)),
        dma((tp - 1,)),
    ]
    anywhere = pl.BlockSpec(memory_space=pl.ANY)
    held = pl.BlockSpec(memory_space=pltpu.VMEM)
    results = pl.pallas_call(
        functools.partial(kernel, kv, tp),
        out_shape=(
            pltpu.VMEM(state.shape, F32),
            pltpu.VMEM((rows, half), BF16),
            pltpu.VMEM((tp - 1, rows, half), BF16),
        ),
        in_specs=[pl.BlockSpec(memory_space=pltpu.HBM)] * 12 + [pl.BlockSpec(memory_space=pltpu.SMEM)],
        out_specs=(held, held, held),
        scratch_shapes=scratch,
        compiler_params=pltpu.CompilerParams(
            collective_id=0, has_side_effects=True, vmem_limit_bytes=VMEM_MIB * 1024 * 1024
        ),
    )(
        tokens,
        w_query,
        w_forget,
        w_input,
        w_gate,
        w_out,
        gain.reshape(1, -1),
        head_gain.reshape(1, -1),
        lower_bound.reshape(1, -1),
        state,
        last_forget,
        last_values,
        accepted,
    )
    return pl.pallas_call(
        finish,
        out_shape=(
            jax.ShapeDtypeStruct((seqs, props, half), BF16),
            jax.ShapeDtypeStruct(state.shape, F32),
        ),
        in_specs=[held] * 3,
        out_specs=(anywhere, anywhere),
        scratch_shapes=[pltpu.VMEM((seqs, props, half), BF16), dma((2,))],
        compiler_params=pltpu.CompilerParams(vmem_limit_bytes=4 * 1024 * 1024),
    )(*results)


def solution(mesh):
    in_specs = (
        P(("grp", "dp"), None, "kv"),
        P("kv", "tp"),
        P("kv", "tp"),
        P("kv", "tp"),
        P("kv", "tp"),
        P("tp", "kv"),
        P(),
        P(),
        P(),
        P(("grp", "dp", "kv"), "tp", None, None),
        P(("grp", "dp", "kv"), None, "tp"),
        P(("grp", "dp", "kv"), None, "tp"),
        P(("grp", "dp", "kv")),
    )
    out_specs = (P(("grp", "dp"), None, ("kv", "tp")), P(("grp", "dp", "kv"), "tp", None, None))
    return jax.shard_map(
        functools.partial(per_device, mesh.shape["kv"], mesh.shape["tp"]),
        mesh=mesh,
        in_specs=in_specs,
        out_specs=out_specs,
        check_vma=False,
    )
```

profile of v0, /device:TPU:1, one launch (start us, length us, event | category | flops | bytes accessed | tf_op | source)
XLA Modules:
  0.0 24.5 jit_solution(634144344994711621)
XLA Ops:
  0.6 22.5 %shard_map.140 = (f32[4,8,128,128]{3,2,1,0:T(8,128)S(1)}, bf16[64,512]{1,0:T(8,128)(2,1)S(1)}, bf16[1,64,512]{2,1,0:T(8,128)(2,1)S(1)}) custom-call(bf16[16,4,1024]{2,1,0:T(4,128)(2,1)} %tokens.1, bf16[1024,1024]{1,0:T(8,128)(2,1)} %w_query.1, bf16[1024,1024]{1,0:T(8,128)(2,1)} %w_forget.1, bf16[1024,1024]{1,0:T(8,128)(2,1)} %w_input.1, ...), custom_call_target="tpu_custom_call" | custom-call | tf_op jit(solution)/shard_map/pallas_call | solution.py:516
  23.2 1.3 %shard_map.141 = (bf16[16,4,512]{2,1,0:T(4,128)(2,1)}, f32[4,8,128,128]{3,2,1,0:T(8,128)}) custom-call(f32[4,8,128,128]{3,2,1,0:T(8,128)S(1)} %get-tuple-element.5.tk_v, bf16[64,512]{1,0:T(8,128)(2,1)S(1)} %get-tuple-element.6.own_v, bf16[1,64,512]{2,1,0:T(8,128)(2,1)S(1)} %get-tuple-element.7.peer_v), custom_call_target="tpu_custom_call" | custom-call | tf_op jit(solution)/shard_map/pallas_call | solution.py:544
where the time goes:
time: 24.8 us; the launch traced here: 24.5 us
  Pallas kernels  23.9 us (96%)
  between operations  0.64 us (3%)
    pallas_call x1, Pallas kernels, per_device(): pl.pallas_call(functools.partial(kernel, kv, tp), out_shape=(pltpu.VMEM(s...  22.5 us
    pallas_call x1, Pallas kernels, per_device(): pl.pallas_call(finish, out_shape=(jax.ShapeDtypeStruct((seqs, props, half...  1.34 us

commit v1 on v0

--- a/solution.py
+++ b/solution.py
@@ -10,12 +10,37 @@
 HEAD = 128
 EPSILON = 1e-05
 CHUNK_HEADS = 4
+LINE = 4
+LINE_HEADS = 2
 VMEM_MIB = 56
 F32 = jnp.float32
 BF16 = jnp.bfloat16
 
-
-def kernel(
+MESSAGES = {
+    "0 for 3": (0, 1, 3, 2),
+    "0 for 2": (0, 1, 2, 3),
+    "0 to 1": (0, 1, 1, 0),
+    "1 to 0": (1, 0, 0, 0),
+    "1 to 3": (1, 3, 3, 0),
+    "1 to 2": (1, 2, 2, 0),
+    "2 to 3": (2, 3, 3, 1),
+    "2 to 0": (2, 0, 0, 1),
+    "2 to 1": (2, 1, 1, 1),
+    "3 for 0": (3, 2, 0, 2),
+    "3 to 1": (3, 1, 1, 4),
+    "3 to 2": (3, 2, 2, 1),
+}
+ORDER = {name: i % 3 for i, name in enumerate(MESSAGES)}
+FIRST = {0: ("0 for 3",), 1: ("1 to 0",), 2: ("2 to 1", "2 to 3"), 3: ("3 for 0",)}
+THEN = {0: ("0 for 2", "0 to 1"), 3: ("3 to 1", "3 to 2")}
+ONWARD = {
+    1: (("0 for 3", "1 to 3"), ("0 for 2", "1 to 2")),
+    2: (("3 for 0", "2 to 0"), None),
+}
+PEERS = ((3, 2, 1), (3, 2, 0), (0, 1, 3), (0, 1, 2))
+
+
+def kernel_any(
     kv,
     tp,
     tokens,
@@ -430,6 +455,439 @@
             copy.wait_send()
 
 
+def kernel_line(
+    tp,
+    tokens,
+    w_query,
+    w_forget,
+    w_input,
+    w_gate,
+    w_out,
+    gain,
+    head_gain,
+    lower_bound,
+    state,
+    last_forget,
+    last_values,
+    accepted,
+    tk_v,
+    own_v,
+    peer_v,
+    tok_v,
+    gain_v,
+    hg_v,
+    lb_v,
+    lf_v,
+    lv_v,
+    rows_v,
+    scaled_v,
+    w_v,
+    wo_v,
+    st_v,
+    tkb_v,
+    lfr_v,
+    lvr_v,
+    ssq_v,
+    ssq_s,
+    ssq_r,
+    prod_v,
+    send_v,
+    recv_v,
+    gath_v,
+    acc_v,
+    part_v,
+    acc_s,
+    load_sem,
+    w_sem,
+    wo_sem,
+    st_sem,
+    ssq_ssem,
+    ssq_rsem,
+    rs_ssem,
+    rs_rsem,
+    ag_ssem,
+    ag_rsem,
+    tp_ssem,
+    tp_rsem,
+    go_sem,
+):
+    kv = LINE
+    me = lax.axis_index("kv")
+    tme = lax.axis_index("tp")
+    seqs, props, feat = tokens.shape
+    own_seqs, heads_dev = state.shape[0], state.shape[1]
+    own_rows = own_seqs * props
+    rows = seqs * props
+    width = gain.shape[1]
+    head_cols = heads_dev * HEAD
+    chunks = heads_dev // LINE_HEADS
+    cw = LINE_HEADS * HEAD
+    half = w_out.shape[1] // tp
+    weights = (w_query, w_forget, w_input, w_gate)
+
+    at_end = jnp.logical_or(me == 0, me == kv - 1)
+
+    def local(src, dst, sem):
+        copy = pltpu.make_async_copy(src, dst, sem)
+        copy.start()
+        return copy
+
+    tok_c = local(tokens, tok_v, load_sem.at[0])
+    gain_c = local(gain, gain_v, load_sem.at[1])
+
+    def load_w(c):
+        return [
+            local(w.at[:, pl.ds(c * cw, cw)], w_v.at[c, :, pl.ds(i * cw, cw)], w_sem.at[c, i])
+            for i, w in enumerate(weights)
+        ]
+
+    def load_late():
+        small = [
+            local(last_forget, lf_v, load_sem.at[2]),
+            local(last_values, lv_v, load_sem.at[3]),
+            local(head_gain, hg_v, load_sem.at[4]),
+            local(lower_bound, lb_v, load_sem.at[5]),
+            local(accepted, acc_s, load_sem.at[6]),
+        ]
+        states = []
+        for c in range(chunks):
+            hs = pl.ds(c * LINE_HEADS, LINE_HEADS)
+            states.append(local(state.at[:, hs], st_v.at[:, hs], st_sem.at[c]))
+        return small, states
+
+    def load_out(o):
+        column = pl.multiple_of(lax.rem(tme + o, tp) * half, half)
+        return local(w_out.at[:, pl.ds(column, half)], wo_v.at[o], wo_sem.at[o])
+
+    w_c = [load_w(0)]
+
+    def signal(axis, peer):
+        pl.semaphore_signal(
+            barrier, inc=1, device_id={axis: peer}, device_id_type=pl.DeviceIdType.MESH
+        )
+
+    barrier = pltpu.get_barrier_semaphore()
+    tp_peers = [lax.rem(tme + o, tp) for o in range(1, tp)]
+    for peer in tp_peers:
+        signal("tp", peer)
+
+    @pl.when(me > 0)
+    def _():
+        signal("kv", me - 1)
+
+    @pl.when(me < kv - 1)
+    def _():
+        signal("kv", me + 1)
+
+    def remote(src, dst, ssem, rsem, axis, peer):
+        return pltpu.make_async_remote_copy(
+            src_ref=src,
+            dst_ref=dst,
+            send_sem=ssem,
+            recv_sem=rsem,
+            device_id={axis: peer},
+            device_id_type=pl.DeviceIdType.MESH,
+        )
+
+    tok_c.wait()
+    gain_c.wait()
+    w_c.append(load_w(1))
+    for s in range(seqs):
+        rows_v[pl.ds(s * props, props), :] = tok_v[s].astype(F32)
+    x = rows_v[...]
+    my_gain = gain_v[:, pl.ds(pl.multiple_of(me * feat, feat), feat)]
+    scaled_v[...] = (x * my_gain).astype(BF16)
+    squared = jnp.sum(x * x, axis=1, keepdims=True)
+    on_row = lax.broadcasted_iota(jnp.int32, (rows, HEAD), 0)
+    on_lane = lax.broadcasted_iota(jnp.int32, (rows, HEAD), 1)
+    along = jnp.sum(jnp.where(on_row == on_lane, squared, 0.0), axis=0, keepdims=True)
+    ssq_v[...] = jnp.broadcast_to(along, ssq_v.shape)
+
+    def rows_of(device):
+        return pl.ds(pl.multiple_of(device * own_rows, own_rows), own_rows)
+
+    def message(c, name):
+        _, to, dest, slot = MESSAGES[name]
+        return remote(
+            send_v.at[c, rows_of(dest)],
+            recv_v.at[c, slot],
+            rs_ssem.at[c, ORDER[name]],
+            rs_rsem.at[c, slot],
+            "kv",
+            to,
+        )
+
+    def pass_on(c, name, onward):
+        _, _, dest, slot = MESSAGES[name]
+        message(c, name).wait_recv()
+        into = rows_of(dest)
+        send_v[c, into, :] = (prod_v[c, into, :] + recv_v[c, slot].astype(F32)).astype(BF16)
+        message(c, onward).start()
+
+    def ssq_copy(i, slot, to):
+        return remote(ssq_s.at[i], ssq_r.at[slot], ssq_ssem.at[i], ssq_rsem.at[slot], "kv", to)
+
+    ssq_s[0] = ssq_v[...]
+    partner = me + 1 - 2 * lax.rem(me, 2)
+    across = jnp.where(me == 1, 2, 1)
+    beyond = jnp.where(me == 1, 3, 0)
+    inside = jnp.logical_not(at_end)
+    pl.semaphore_wait(barrier, jnp.where(at_end, tp, tp + 1))
+    ssq_copy(0, 0, partner).start()
+
+    @pl.when(inside)
+    def _():
+        pl.semaphore_signal(
+            go_sem, inc=1, device_id={"kv": across}, device_id_type=pl.DeviceIdType.MESH
+        )
+
+    @pl.when(me == 2)
+    def _():
+        pl.semaphore_signal(
+            go_sem, inc=1, device_id={"kv": 3}, device_id_type=pl.DeviceIdType.MESH
+        )
+
+    @pl.when(me != 1)
+    def _():
+        recv_v[:, 4] = jnp.zeros_like(recv_v[:, 4])
+
+    place = lax.broadcasted_iota(jnp.int32, (own_rows, 1), 0)
+    prop = lax.rem(place, props)
+    seq = place // props
+
+    def old_terms():
+        for copy in small_c:
+            copy.wait()
+        for s in range(own_seqs):
+            lfr_v[pl.ds(s * props, props), :] = lf_v[s]
+            lvr_v[pl.ds(s * props, props), :] = lv_v[s].astype(F32)
+        limit = jnp.zeros((own_rows, 1), jnp.int32)
+        for s in range(own_seqs):
+            limit = jnp.where(seq == s, acc_s[s], limit)
+        mask = prop < limit
+        old = lfr_v[...]
+        decay = jnp.where(mask, old, 1.0)
+        weight = jnp.where(mask, 1.0 - old, 0.0)
+        after = jnp.ones_like(decay)
+        for lag in range(1, props):
+            after = after * jnp.where(
+                prop < props - lag, pltpu.roll(decay, own_rows - lag, 0), 1.0
+            )
+        return decay * after, weight * after, lvr_v[...].astype(BF16)
+
+    def take(c, ends, old_weight, old_values):
+        st_c[c].wait()
+        lane_seq = lax.broadcasted_iota(jnp.int32, (1, own_rows), 1) // props
+        for h in range(c * LINE_HEADS, (c + 1) * LINE_HEADS):
+            cols = slice(h * HEAD, (h + 1) * HEAD)
+            end_t = ends[:, cols].T
+            weight_t = old_weight[:, cols].T
+            for s in range(own_seqs):
+                mine = jnp.where(lane_seq == s, weight_t, 0.0).astype(BF16)
+                added = jnp.dot(mine, old_values[:, cols], preferred_element_type=F32)
+                new = end_t[:, s * props : s * props + 1] * st_v[s, h] + added
+                tk_v[s, h] = new
+                tkb_v[h, pl.ds(s * HEAD, HEAD), :] = new.astype(BF16)
+
+    for c in range(chunks):
+        for copy in w_c[c]:
+            copy.wait()
+        if c + 2 < chunks:
+            w_c.append(load_w(c + 2))
+        elif c + 2 == chunks:
+            small_c, st_c = load_late()
+        else:
+            wo_c = [load_out(o) for o in range(tp)]
+        product = jnp.dot(scaled_v[...], w_v[c], preferred_element_type=F32)
+        prod_v[c] = product
+        send_v[c] = product.astype(BF16)
+
+        for device, names in FIRST.items():
+
+            @pl.when(me == device)
+            def _():
+                for name in names:
+                    message(c, name).start()
+
+    for device, names in THEN.items():
+
+        @pl.when(me == device)
+        def _():
+            if device == 3:
+                pl.semaphore_wait(go_sem, 1)
+            for name in names:
+                for c in range(chunks):
+                    message(c, name).start()
+
+    terms = old_terms()
+    ssq_copy(0, 0, partner).wait_recv()
+
+    @pl.when(inside)
+    def _():
+        pl.semaphore_wait(go_sem, 1)
+        ssq_s[1] = ssq_v[...] + ssq_r[0]
+        ssq_copy(1, 1, across).start()
+        ssq_s[2] = ssq_v[...] + ssq_r[0]
+        ssq_copy(2, 1, beyond).start()
+
+    for c in range(chunks):
+        for device, steps in ONWARD.items():
+
+            @pl.when(me == device)
+            def _():
+                pass_on(c, *steps[0])
+
+        take(c, *terms)
+
+    @pl.when(me == 1)
+    def _():
+        for c in range(chunks):
+            pass_on(c, *ONWARD[1][1])
+
+    ssq_copy(1, 1, partner).wait_recv()
+    whole = ssq_v[...] + ssq_r[0] + ssq_r[1]
+    mine_rows = rows_of(me)
+    picked = lax.broadcasted_iota(jnp.int32, (own_rows, HEAD), 1) == (
+        lax.broadcasted_iota(jnp.int32, (own_rows, HEAD), 0) + me * own_rows
+    )
+    squares = jnp.sum(jnp.where(picked, whole[:1], 0.0), axis=1, keepdims=True)
+    row_scale = lax.rsqrt(squares / width + EPSILON)
+    peers = [
+        functools.reduce(lambda found, d: jnp.where(me == d, PEERS[d][o], found), range(kv), 0)
+        for o in range(kv - 1)
+    ]
+
+    def head_copy(c, o):
+        return remote(
+            gath_v.at[c, mine_rows],
+            gath_v.at[c, mine_rows],
+            ag_ssem.at[c, o],
+            ag_rsem.at[c, me],
+            "kv",
+            peers[o],
+        )
+
+    def recur(c):
+        for slot in range(2):
+            remote(
+                send_v.at[c, mine_rows], recv_v.at[c, slot], rs_ssem.at[c, 0],
+                rs_rsem.at[c, slot], "kv", peers[0],
+            ).wait_recv()
+
+        @pl.when(me == 1)
+        def _():
+            message(c, "3 to 1").wait_recv()
+
+        def projected(i):
+            cols = pl.ds(i * cw, cw)
+            total = prod_v[c, mine_rows, cols]
+            for slot in (0, 1, 4):
+                total = total + recv_v[c, slot, :, cols].astype(F32)
+            return total * row_scale
+
+        column = pl.multiple_of(tme * head_cols + c * cw, cw)
+        floor_gate = lb_v[:, pl.ds(column, cw)]
+        forget = floor_gate + (1.0 - floor_gate) * jax.nn.sigmoid(projected(1))
+        keys = 1.0 - forget
+        queries = jax.nn.silu(projected(0)) * HEAD ** (-0.5)
+        values = projected(2)
+        gate = jax.nn.silu(projected(3)) * hg_v[:, pl.ds(column, cw)]
+        start = forget
+        for lag in range(1, props):
+            start = start * jnp.where(prop >= lag, pltpu.roll(forget, lag, 0), 1.0)
+        reading = queries * start
+        results = []
+        for h in range(LINE_HEADS):
+            cols = slice(h * HEAD, (h + 1) * HEAD)
+            lhs = jnp.concatenate(
+                [jnp.where(seq == s, reading[:, cols], 0.0) for s in range(own_seqs)], axis=1
+            ).astype(BF16)
+            results.append(
+                jnp.dot(lhs, tkb_v[c * LINE_HEADS + h], preferred_element_type=F32)
+            )
+        decay = queries
+        for lag in range(props):
+            if lag > 0:
+                decay = decay * (forget if lag == 1 else pltpu.roll(forget, lag - 1, 0))
+            pair = decay * (keys if lag == 0 else pltpu.roll(keys, lag, 0))
+            pair = jnp.where(prop >= lag, pair, 0.0)
+            moved = values if lag == 0 else pltpu.roll(values, lag, 0)
+            for h in range(LINE_HEADS):
+                cols = slice(h * HEAD, (h + 1) * HEAD)
+                score = jnp.sum(pair[:, cols], axis=1, keepdims=True)
+                results[h] = results[h] + score * moved[:, cols]
+        outs = []
+        for h in range(LINE_HEADS):
+            cols = slice(h * HEAD, (h + 1) * HEAD)
+            r = results[h]
+            normed = r * lax.rsqrt(jnp.mean(r * r, axis=1, keepdims=True) + EPSILON)
+            outs.append((normed * gate[:, cols]).astype(BF16))
+        gath_v[c, mine_rows, :] = jnp.concatenate(outs, axis=1)
+        for o in range(kv - 1):
+            head_copy(c, o).start()
+
+    def product_of(c, o):
+        term = jnp.dot(
+            gath_v[c], wo_v[o, pl.ds(c * cw, cw), :], preferred_element_type=F32
+        )
+        return term if c == 0 else acc_v[o] + term
+
+    def gathered(c):
+        for peer in peers:
+            theirs = gath_v.at[c, rows_of(peer)]
+            remote(
+                theirs, theirs, ag_ssem.at[c, 0], ag_rsem.at[c, peer], "kv", peer
+            ).wait_recv()
+
+    for c in range(chunks):
+        recur(c)
+    for copy in wo_c:
+        copy.wait()
+    for c in range(chunks - 1):
+        gathered(c)
+        for o in range(tp):
+            acc_v[o] = product_of(c, o)
+    gathered(chunks - 1)
+    tp_c = []
+    for o in range(1, tp):
+        part_v[o - 1] = product_of(chunks - 1, o).astype(BF16)
+        copy = remote(
+            part_v.at[o - 1],
+            peer_v.at[o - 1],
+            tp_ssem.at[o - 1],
+            tp_rsem.at[o - 1],
+            "tp",
+            tp_peers[o - 1],
+        )
+        copy.start()
+        tp_c.append(copy)
+    own_v[...] = product_of(chunks - 1, 0).astype(BF16)
+    for copy in tp_c:
+        copy.wait_recv()
+
+    for device in range(kv):
+
+        @pl.when(me == device)
+        def _():
+            for name, (sender, _, _, _) in MESSAGES.items():
+                if sender == device:
+                    for c in range(chunks):
+                        message(c, name).wait_send()
+
+    ssq_copy(0, 0, partner).wait_send()
+
+    @pl.when(inside)
+    def _():
+        ssq_copy(1, 1, across).wait_send()
+        ssq_copy(2, 1, beyond).wait_send()
+
+    for c in range(chunks):
+        for o in range(kv - 1):
+            head_copy(c, o).wait_send()
+    for copy in tp_c:
+        copy.wait_send()
+
+
 def finish(tk_v, own_v, peer_v, mixed, taken, mix_v, sem):
     tk_c = pltpu.make_async_copy(tk_v, taken, sem.at[0])
     tk_c.start()
@@ -467,8 +925,10 @@
     own_rows = own_seqs * props
     rows = seqs * props
     head_cols = heads_dev * HEAD
-    chunks = heads_dev // CHUNK_HEADS
-    cw = CHUNK_HEADS * HEAD
+    on_line = kv == LINE and rows <= HEAD
+    per_chunk = LINE_HEADS if on_line else CHUNK_HEADS
+    chunks = heads_dev // per_chunk
+    cw = per_chunk * HEAD
     half = w_out.shape[1] // tp
     peers = kv - 1
     dma = pltpu.SemaphoreType.DMA
@@ -487,40 +947,72 @@
         pltpu.VMEM((heads_dev, own_seqs * HEAD, HEAD), BF16),
         pltpu.VMEM((own_rows, head_cols), F32),
         pltpu.VMEM((own_rows, head_cols), F32),
-        pltpu.VMEM((rows, HEAD), F32),
-        pltpu.VMEM((peers, own_rows, HEAD), F32),
-        pltpu.VMEM((chunks, rows, 4 * cw), F32),
-        pltpu.VMEM((chunks, rows, 4 * cw), BF16),
-        pltpu.VMEM((chunks, peers, own_rows, 4 * cw), BF16),
-        pltpu.VMEM((chunks, rows, cw), BF16),
-        pltpu.VMEM((tp, rows, half), F32),
-        pltpu.VMEM((tp - 1, rows, half), BF16),
-        pltpu.VMEM((chunks, own_rows, 4 * cw), BF16),
-        dma((6,)),
-        dma((chunks, 4)),
-        dma((tp,)),
-        dma((chunks,)),
-        dma((peers,)),
-        dma((peers,)),
-        dma((chunks, peers)),
-        dma((chunks, peers)),
-        dma((chunks,)),
-        dma((chunks,)),
-        dma((chunks, peers)),
-        dma((chunks, peers)),
-        dma((tp - 1,)),
-        dma((tp - 1,)),
     ]
+    if on_line:
+        body = functools.partial(kernel_line, tp)
+        scratch += [
+            pltpu.VMEM((1, HEAD), F32),
+            pltpu.VMEM((3, 1, HEAD), F32),
+            pltpu.VMEM((2, 1, HEAD), F32),
+            pltpu.VMEM((chunks, rows, 4 * cw), F32),
+            pltpu.VMEM((chunks, rows, 4 * cw), BF16),
+            pltpu.VMEM((chunks, 5, own_rows, 4 * cw), BF16),
+            pltpu.VMEM((chunks, rows, cw), BF16),
+            pltpu.VMEM((tp, rows, half), F32),
+            pltpu.VMEM((tp - 1, rows, half), BF16),
+            pltpu.SMEM((own_seqs,), jnp.int32),
+            dma((7,)),
+            dma((chunks, 4)),
+            dma((tp,)),
+            dma((chunks,)),
+            dma((3,)),
+            dma((2,)),
+            dma((chunks, 3)),
+            dma((chunks, 5)),
+            dma((chunks, peers)),
+            dma((chunks, kv)),
+            dma((tp - 1,)),
+            dma((tp - 1,)),
+            pltpu.SemaphoreType.REGULAR,
+        ]
+    else:
+        body = functools.partial(kernel_any, kv, tp)
+        scratch += [
+            pltpu.VMEM((rows, HEAD), F32),
+            pltpu.VMEM((peers, own_rows, HEAD), F32),
+            pltpu.VMEM((chunks, rows, 4 * cw), F32),
+            pltpu.VMEM((chunks, rows, 4 * cw), BF16),
+            pltpu.VMEM((chunks, peers, own_rows, 4 * cw), BF16),
+            pltpu.VMEM((chunks, rows, cw), BF16),
+            pltpu.VMEM((tp, rows, half), F32),
+            pltpu.VMEM((tp - 1, rows, half), BF16),
+            pltpu.VMEM((chunks, own_rows, 4 * cw), BF16),
+            dma((6,)),
+            dma((chunks, 4)),
+            dma((tp,)),
+            dma((chunks,)),
+            dma((peers,)),
+            dma((peers,)),
+            dma((chunks, peers)),
+            dma((chunks, peers)),
+            dma((chunks,)),
+            dma((chunks,)),
+            dma((chunks, peers)),
+            dma((chunks, peers)),
+            dma((tp - 1,)),
+            dma((tp - 1,)),
+        ]
     anywhere = pl.BlockSpec(memory_space=pl.ANY)
     held = pl.BlockSpec(memory_space=pltpu.VMEM)
     results = pl.pallas_call(
-        functools.partial(kernel, kv, tp),
+        body,
         out_shape=(
             pltpu.VMEM(state.shape, F32),
             pltpu.VMEM((rows, half), BF16),
             pltpu.VMEM((tp - 1, rows, half), BF16),
         ),
-        in_specs=[pl.BlockSpec(memory_space=pltpu.HBM)] * 12 + [pl.BlockSpec(memory_space=pltpu.SMEM)],
+        in_specs=[pl.BlockSpec(memory_space=pltpu.HBM)] * 12
+        + [pl.BlockSpec(memory_space=pltpu.HBM if on_line else pltpu.SMEM)],
         out_specs=(held, held, held),
         scratch_shapes=scratch,
         compiler_params=pltpu.CompilerParams(

time: 24.8 us -> 24.6 us (level)
  no operation moved by 1% of the time
where the time goes in v1:
time: 24.6 us; the launch traced here: 24.4 us
  Pallas kernels  23.7 us (96%)
  between operations  0.64 us (3%)
    pallas_call x1, Pallas kernels, per_device(): pl.pallas_call(body, out_shape=(pltpu.VMEM(state.shape, F32), pltpu.VMEM(...  22.4 us
    pallas_call x1, Pallas kernels, per_device(): pl.pallas_call(finish, out_shape=(jax.ShapeDtypeStruct((seqs, props, half...  1.34 us

profile of v1, /device:TPU:1, one launch (start us, length us, event | category | flops | bytes accessed | tf_op | source)
XLA Modules:
  0.0 24.4 jit_solution(8484916476495566893)
XLA Ops:
  0.6 22.4 %shard_map.140 = (f32[4,8,128,128]{3,2,1,0:T(8,128)S(1)}, bf16[64,512]{1,0:T(8,128)(2,1)S(1)}, bf16[1,64,512]{2,1,0:T(8,128)(2,1)S(1)}) custom-call(bf16[16,4,1024]{2,1,0:T(4,128)(2,1)} %tokens.1, bf16[1024,1024]{1,0:T(8,128)(2,1)} %w_query.1, bf16[1024,1024]{1,0:T(8,128)(2,1)} %w_forget.1, bf16[1024,1024]{1,0:T(8,128)(2,1)} %w_input.1, ...), custom_call_target="tpu_custom_call" | custom-call | tf_op jit(solution)/shard_map/pallas_call | solution.py:1007
  23.0 1.3 %shard_map.141 = (bf16[16,4,512]{2,1,0:T(4,128)(2,1)}, f32[4,8,128,128]{3,2,1,0:T(8,128)}) custom-call(f32[4,8,128,128]{3,2,1,0:T(8,128)S(1)} %get-tuple-element.5.tk_v, bf16[64,512]{1,0:T(8,128)(2,1)S(1)} %get-tuple-element.6.own_v, bf16[1,64,512]{2,1,0:T(8,128)(2,1)S(1)} %get-tuple-element.7.peer_v), custom_call_target="tpu_custom_call" | custom-call | tf_op jit(solution)/shard_map/pallas_call | solution.py:1036

commit v2 on v1

--- a/solution.py
+++ b/solution.py
@@ -12,13 +12,14 @@
 CHUNK_HEADS = 4
 LINE = 4
 LINE_HEADS = 2
+CROSS = 1
 VMEM_MIB = 56
 F32 = jnp.float32
 BF16 = jnp.bfloat16
 
 MESSAGES = {
-    "0 for 3": (0, 1, 3, 2),
-    "0 for 2": (0, 1, 2, 3),
+    "0 for 3": (0, 1, 3, 3),
+    "0 for 2": (0, 1, 2, 4),
     "0 to 1": (0, 1, 1, 0),
     "1 to 0": (1, 0, 0, 0),
     "1 to 3": (1, 3, 3, 0),
@@ -26,11 +27,11 @@
     "2 to 3": (2, 3, 3, 1),
     "2 to 0": (2, 0, 0, 1),
     "2 to 1": (2, 1, 1, 1),
-    "3 for 0": (3, 2, 0, 2),
-    "3 to 1": (3, 1, 1, 4),
+    "3 for 0": (3, 2, 0, 3),
+    "3 to 1": (3, 1, 1, 2),
     "3 to 2": (3, 2, 2, 1),
 }
-ORDER = {name: i % 3 for i, name in enumerate(MESSAGES)}
+OWN = 3
 FIRST = {0: ("0 for 3",), 1: ("1 to 0",), 2: ("2 to 1", "2 to 3"), 3: ("3 for 0",)}
 THEN = {0: ("0 for 2", "0 to 1"), 3: ("3 to 1", "3 to 2")}
 ONWARD = {
@@ -471,8 +472,9 @@
     last_values,
     accepted,
     tk_v,
-    own_v,
-    peer_v,
+    acc_v,
+    last_v,
+    wl_v,
     tok_v,
     gain_v,
     hg_v,
@@ -494,8 +496,6 @@
     send_v,
     recv_v,
     gath_v,
-    acc_v,
-    part_v,
     acc_s,
     load_sem,
     w_sem,
@@ -507,8 +507,11 @@
     rs_rsem,
     ag_ssem,
     ag_rsem,
-    tp_ssem,
-    tp_rsem,
+    cross_rsem,
+    fw_ssem,
+    fw_rsem,
+    wo_ssem,
+    wo_rsem,
     go_sem,
 ):
     kv = LINE
@@ -535,11 +538,12 @@
     tok_c = local(tokens, tok_v, load_sem.at[0])
     gain_c = local(gain, gain_v, load_sem.at[1])
 
+    def held(ref, sem):
+        pltpu.make_async_copy(ref, ref, sem).wait()
+
     def load_w(c):
-        return [
-            local(w.at[:, pl.ds(c * cw, cw)], w_v.at[c, :, pl.ds(i * cw, cw)], w_sem.at[c, i])
-            for i, w in enumerate(weights)
-        ]
+        for i, w in enumerate(weights):
+            local(w.at[:, pl.ds(c * cw, cw)], w_v.at[c, :, pl.ds(i * cw, cw)], w_sem.at[c])
 
     def load_late():
         small = [
@@ -549,17 +553,20 @@
             local(lower_bound, lb_v, load_sem.at[5]),
             local(accepted, acc_s, load_sem.at[6]),
         ]
-        states = []
-        for c in range(chunks):
-            hs = pl.ds(c * LINE_HEADS, LINE_HEADS)
-            states.append(local(state.at[:, hs], st_v.at[:, hs], st_sem.at[c]))
-        return small, states
-
-    def load_out(o):
-        column = pl.multiple_of(lax.rem(tme + o, tp) * half, half)
-        return local(w_out.at[:, pl.ds(column, half)], wo_v.at[o], wo_sem.at[o])
-
-    w_c = [load_w(0)]
+        return small, local(state, st_v, st_sem)
+
+    split = (chunks - 1) * cw
+    crossed = chunks - CROSS
+
+    def load_out():
+        cols = pl.ds(pl.multiple_of(tme * half, half), half)
+        local(w_out.at[:split, cols], wo_v.at[0], wo_sem)
+        local(w_out.at[split:, cols], wl_v.at[0], wo_sem)
+
+    def out_held(sem):
+        held(w_v.at[0, : head_cols * half // (4 * cw)], sem)
+
+    load_w(0)
 
     def signal(axis, peer):
         pl.semaphore_signal(
@@ -591,7 +598,8 @@
 
     tok_c.wait()
     gain_c.wait()
-    w_c.append(load_w(1))
+    load_w(1)
+    load_w(2)
     for s in range(seqs):
         rows_v[pl.ds(s * props, props), :] = tok_v[s].astype(F32)
     x = rows_v[...]
@@ -611,8 +619,8 @@
         return remote(
             send_v.at[c, rows_of(dest)],
             recv_v.at[c, slot],
-            rs_ssem.at[c, ORDER[name]],
-            rs_rsem.at[c, slot],
+            rs_ssem,
+            rs_rsem.at[c, max(slot - OWN + 1, 0)],
             "kv",
             to,
         )
@@ -649,7 +657,7 @@
 
     @pl.when(me != 1)
     def _():
-        recv_v[:, 4] = jnp.zeros_like(recv_v[:, 4])
+        recv_v[:, OWN - 1] = jnp.zeros_like(recv_v[:, OWN - 1])
 
     place = lax.broadcasted_iota(jnp.int32, (own_rows, 1), 0)
     prop = lax.rem(place, props)
@@ -676,7 +684,8 @@
         return decay * after, weight * after, lvr_v[...].astype(BF16)
 
     def take(c, ends, old_weight, old_values):
-        st_c[c].wait()
+        if c == 0:
+            st_c.wait()
         lane_seq = lax.broadcasted_iota(jnp.int32, (1, own_rows), 1) // props
         for h in range(c * LINE_HEADS, (c + 1) * LINE_HEADS):
             cols = slice(h * HEAD, (h + 1) * HEAD)
@@ -690,14 +699,13 @@
                 tkb_v[h, pl.ds(s * HEAD, HEAD), :] = new.astype(BF16)
 
     for c in range(chunks):
-        for copy in w_c[c]:
-            copy.wait()
-        if c + 2 < chunks:
-            w_c.append(load_w(c + 2))
+        held(w_v.at[c], w_sem.at[c])
+        if c + 3 < chunks:
+            load_w(c + 3)
+        elif c + 3 == chunks:
+            small_c, st_c = load_late()
         elif c + 2 == chunks:
-            small_c, st_c = load_late()
-        else:
-            wo_c = [load_out(o) for o in range(tp)]
+            load_out()
         product = jnp.dot(scaled_v[...], w_v[c], preferred_element_type=F32)
         prod_v[c] = product
         send_v[c] = product.astype(BF16)
@@ -743,6 +751,15 @@
     def _():
         for c in range(chunks):
             pass_on(c, *ONWARD[1][1])
+
+    for o in range(1, tp):
+        cols = pl.ds(pl.multiple_of(tp_peers[o - 1] * half, half), half)
+        for rows_out, into in ((w_out.at[:split, cols], wo_v), (w_out.at[split:, cols], wl_v)):
+            copy = remote(
+                rows_out, into.at[tp - o], wo_ssem.at[o - 1], wo_rsem.at[tp - o - 1],
+                "tp", tp_peers[o - 1],
+            )
+            copy.start()
 
     ssq_copy(1, 1, partner).wait_recv()
     whole = ssq_v[...] + ssq_r[0] + ssq_r[1]
@@ -757,31 +774,48 @@
         for o in range(kv - 1)
     ]
 
+    def heads_of(c, slot):
+        return gath_v.at[slot, c] if c < chunks - 1 else last_v.at[slot]
+
     def head_copy(c, o):
+        mine = heads_of(c, 0).at[mine_rows]
+        return remote(mine, mine, ag_ssem, ag_rsem.at[c], "kv", peers[o])
+
+    def cross_copy(c, o, i):
+        ids = {"tp": tp_peers[o - 1]}
+        if i < kv - 1:
+            ids["kv"] = peers[i]
+        return pltpu.make_async_remote_copy(
+            src_ref=heads_of(c, 0).at[mine_rows],
+            dst_ref=heads_of(c, tp - o).at[mine_rows],
+            send_sem=ag_ssem,
+            recv_sem=cross_rsem.at[c - crossed, tp - o - 1],
+            device_id=ids,
+            device_id_type=pl.DeviceIdType.MESH,
+        )
+
+    def cross_copies(c):
+        return [cross_copy(c, o, i) for o in range(1, tp) for i in range(kv)]
+
+    def forward(c, o):
         return remote(
-            gath_v.at[c, mine_rows],
-            gath_v.at[c, mine_rows],
-            ag_ssem.at[c, o],
-            ag_rsem.at[c, me],
-            "kv",
-            peers[o],
+            gath_v.at[0, c], gath_v.at[tp - o, c], fw_ssem.at[c, o - 1],
+            fw_rsem.at[c, tp - o - 1], "tp", tp_peers[o - 1],
         )
 
     def recur(c):
-        for slot in range(2):
-            remote(
-                send_v.at[c, mine_rows], recv_v.at[c, slot], rs_ssem.at[c, 0],
-                rs_rsem.at[c, slot], "kv", peers[0],
-            ).wait_recv()
-
         @pl.when(me == 1)
         def _():
-            message(c, "3 to 1").wait_recv()
+            held(recv_v.at[c, :OWN], rs_rsem.at[c, 0])
+
+        @pl.when(me != 1)
+        def _():
+            held(recv_v.at[c, : OWN - 1], rs_rsem.at[c, 0])
 
         def projected(i):
             cols = pl.ds(i * cw, cw)
             total = prod_v[c, mine_rows, cols]
-            for slot in (0, 1, 4):
+            for slot in range(OWN):
                 total = total + recv_v[c, slot, :, cols].astype(F32)
             return total * row_scale
 
@@ -822,58 +856,48 @@
             r = results[h]
             normed = r * lax.rsqrt(jnp.mean(r * r, axis=1, keepdims=True) + EPSILON)
             outs.append((normed * gate[:, cols]).astype(BF16))
-        gath_v[c, mine_rows, :] = jnp.concatenate(outs, axis=1)
+        heads_of(c, 0)[mine_rows, :] = jnp.concatenate(outs, axis=1)
         for o in range(kv - 1):
             head_copy(c, o).start()
-
-    def product_of(c, o):
+        if c >= crossed:
+            for copy in cross_copies(c):
+                copy.start()
+
+    def gathered(c):
+        held(heads_of(c, 0).at[: (kv - 1) * own_rows], ag_rsem.at[c])
+
+    def product_of(c, slot):
         term = jnp.dot(
-            gath_v[c], wo_v[o, pl.ds(c * cw, cw), :], preferred_element_type=F32
-        )
-        return term if c == 0 else acc_v[o] + term
-
-    def gathered(c):
-        for peer in peers:
-            theirs = gath_v.at[c, rows_of(peer)]
-            remote(
-                theirs, theirs, ag_ssem.at[c, 0], ag_rsem.at[c, peer], "kv", peer
-            ).wait_recv()
+            gath_v[slot, c], wo_v[slot, pl.ds(c * cw, cw), :], preferred_element_type=F32
+        )
+        acc_v[slot] = term if c == 0 else acc_v[slot] + term
+
+    def from_tp(c):
+        for o in range(1, tp):
+            if c < crossed:
+                forward(c, tp - o).wait_recv()
+                continue
+            held(heads_of(c, o), cross_rsem.at[c - crossed, o - 1])
 
     for c in range(chunks):
         recur(c)
-    for copy in wo_c:
-        copy.wait()
-    for c in range(chunks - 1):
+    out_held(wo_sem)
+    for o in range(1, tp):
+        out_held(wo_rsem.at[o - 1])
+    for c in range(chunks):
         gathered(c)
-        for o in range(tp):
-            acc_v[o] = product_of(c, o)
-    gathered(chunks - 1)
-    tp_c = []
-    for o in range(1, tp):
-        part_v[o - 1] = product_of(chunks - 1, o).astype(BF16)
-        copy = remote(
-            part_v.at[o - 1],
-            peer_v.at[o - 1],
-            tp_ssem.at[o - 1],
-            tp_rsem.at[o - 1],
-            "tp",
-            tp_peers[o - 1],
-        )
-        copy.start()
-        tp_c.append(copy)
-    own_v[...] = product_of(chunks - 1, 0).astype(BF16)
-    for copy in tp_c:
-        copy.wait_recv()
-
-    for device in range(kv):
-
-        @pl.when(me == device)
-        def _():
-            for name, (sender, _, _, _) in MESSAGES.items():
-                if sender == device:
-                    for c in range(chunks):
-                        message(c, name).wait_send()
-
+        if c < crossed:
+            for o in range(1, tp):
+                forward(c, o).start()
+        if c < chunks - 1:
+            product_of(c, 0)
+        if c > 0:
+            from_tp(c - 1)
+            for o in range(1, tp):
+                product_of(c - 1, o)
+    from_tp(chunks - 1)
+
+    held(send_v.at[:, : (kv - 1) * own_rows], rs_ssem)
     ssq_copy(0, 0, partner).wait_send()
 
     @pl.when(inside)
@@ -881,11 +905,29 @@
         ssq_copy(1, 1, across).wait_send()
         ssq_copy(2, 1, beyond).wait_send()
 
-    for c in range(chunks):
-        for o in range(kv - 1):
-            head_copy(c, o).wait_send()
-    for copy in tp_c:
-        copy.wait_send()
+    blocks = chunks * (kv - 1) + CROSS * (tp - 1) * kv
+    held(w_v.at[0, : blocks * own_rows // 4], ag_ssem)
+    for o in range(1, tp):
+        out_held(wo_ssem.at[o - 1])
+    for c in range(crossed):
+        for o in range(1, tp):
+            forward(c, o).wait_send()
+
+
+def finish_line(tk_v, acc_v, last_v, wl_v, mixed, taken, mix_v, sem):
+    tk_c = pltpu.make_async_copy(tk_v, taken, sem.at[0])
+    tk_c.start()
+    seqs, props, _ = mixed.shape
+    total = 0.0
+    for slot in range(acc_v.shape[0]):
+        term = jnp.dot(last_v[slot], wl_v[slot], preferred_element_type=F32)
+        total = total + (acc_v[slot] + term).astype(BF16).astype(F32)
+    for s in range(seqs):
+        mix_v[s] = total[s * props : (s + 1) * props].astype(BF16)
+    mix_c = pltpu.make_async_copy(mix_v, mixed, sem.at[1])
+    mix_c.start()
+    mix_c.wait()
+    tk_c.wait()
 
 
 def finish(tk_v, own_v, peer_v, mixed, taken, mix_v, sem):
@@ -949,7 +991,14 @@
         pltpu.VMEM((own_rows, head_cols), F32),
     ]
     if on_line:
-        body = functools.partial(kernel_line, tp)
+        body, last = functools.partial(kernel_line, tp), finish_line
+        scratch[9] = pltpu.VMEM((tp, head_cols - cw, half), BF16)
+        outs = (
+            pltpu.VMEM(state.shape, F32),
+            pltpu.VMEM((tp, rows, half), F32),
+            pltpu.VMEM((tp, rows, cw), BF16),
+            pltpu.VMEM((tp, cw, half), BF16),
+        )
         scratch += [
             pltpu.VMEM((1, HEAD), F32),
             pltpu.VMEM((3, 1, HEAD), F32),
@@ -957,26 +1006,32 @@
             pltpu.VMEM((chunks, rows, 4 * cw), F32),
             pltpu.VMEM((chunks, rows, 4 * cw), BF16),
             pltpu.VMEM((chunks, 5, own_rows, 4 * cw), BF16),
-            pltpu.VMEM((chunks, rows, cw), BF16),
-            pltpu.VMEM((tp, rows, half), F32),
-            pltpu.VMEM((tp - 1, rows, half), BF16),
+            pltpu.VMEM((tp, chunks - 1, rows, cw), BF16),
             pltpu.SMEM((own_seqs,), jnp.int32),
             dma((7,)),
-            dma((chunks, 4)),
-            dma((tp,)),
             dma((chunks,)),
+            dma,
+            dma,
             dma((3,)),
             dma((2,)),
+            dma,
             dma((chunks, 3)),
-            dma((chunks, 5)),
-            dma((chunks, peers)),
-            dma((chunks, kv)),
+            dma,
+            dma((chunks,)),
+            dma((CROSS, tp - 1)),
+            dma((chunks - CROSS, tp - 1)),
+            dma((chunks - CROSS, tp - 1)),
             dma((tp - 1,)),
             dma((tp - 1,)),
             pltpu.SemaphoreType.REGULAR,
         ]
     else:
-        body = functools.partial(kernel_any, kv, tp)
+        body, last = functools.partial(kernel_any, kv, tp), finish
+        outs = (
+            pltpu.VMEM(state.shape, F32),
+            pltpu.VMEM((rows, half), BF16),
+            pltpu.VMEM((tp - 1, rows, half), BF16),
+        )
         scratch += [
             pltpu.VMEM((rows, HEAD), F32),
             pltpu.VMEM((peers, own_rows, HEAD), F32),
@@ -1006,14 +1061,10 @@
     held = pl.BlockSpec(memory_space=pltpu.VMEM)
     results = pl.pallas_call(
         body,
-        out_shape=(
-            pltpu.VMEM(state.shape, F32),
-            pltpu.VMEM((rows, half), BF16),
-            pltpu.VMEM((tp - 1, rows, half), BF16),
-        ),
+        out_shape=outs,
         in_specs=[pl.BlockSpec(memory_space=pltpu.HBM)] * 12
         + [pl.BlockSpec(memory_space=pltpu.HBM if on_line else pltpu.SMEM)],
-        out_specs=(held, held, held),
+        out_specs=(held,) * len(outs),
         scratch_shapes=scratch,
         compiler_params=pltpu.CompilerParams(
             collective_id=0, has_side_effects=True, vmem_limit_bytes=VMEM_MIB * 1024 * 1024
@@ -1034,12 +1085,12 @@
         accepted,
     )
     return pl.pallas_call(
-        finish,
+        last,
         out_shape=(
             jax.ShapeDtypeStruct((seqs, props, half), BF16),
             jax.ShapeDtypeStruct(state.shape, F32),
         ),
-        in_specs=[held] * 3,
+        in_specs=[held] * len(outs),
         out_specs=(anywhere, anywhere),
         scratch_shapes=[pltpu.VMEM((seqs, props, half), BF16), dma((2,))],
         compiler_params=pltpu.CompilerParams(vmem_limit_bytes=4 * 1024 * 1024),

time: 24.6 us -> 23.5 us (0.955)
  Pallas kernels: 23.7 us -> 22.8 us
    pallas_call x2, Pallas kernels: 23.7 us -> 22.8 us  [the longest x1 21.4 us: per_device(): pl.pallas_call(body, out_shape=outs, in_specs=[pl.BlockSpec(memory_space=...]
where the time goes in v2:
time: 23.5 us; the launch traced here: 23.4 us
  Pallas kernels  22.8 us (97%)
  between operations  0.64 us (3%)
    pallas_call x1, Pallas kernels, per_device(): pl.pallas_call(body, out_shape=outs, in_specs=[pl.BlockSpec(memory_space=...  21.4 us
    pallas_call x1, Pallas kernels, per_device(): pl.pallas_call(last, out_shape=(jax.ShapeDtypeStruct((seqs, props, half),...  1.36 us

profile of v2, /device:TPU:1, one launch (start us, length us, event | category | flops | bytes accessed | tf_op | source)
XLA Modules:
  0.0 23.4 jit_solution(16906135293603512547)
XLA Ops:
  0.6 21.4 %shard_map.140 = (f32[4,8,128,128]{3,2,1,0:T(8,128)S(1)}, f32[2,64,512]{2,1,0:T(8,128)S(1)}, bf16[2,64,256]{2,1,0:T(8,128)(2,1)S(1)}, bf16[2,256,512]{2,1,0:T(8,128)(2,1)S(1)}) custom-call(bf16[16,4,1024]{2,1,0:T(4,128)(2,1)} %tokens.1, bf16[1024,1024]{1,0:T(8,128)(2,1)} %w_query.1, bf16[1024,1024]{1,0:T(8,128)(2,1)} %w_forget.1, ...), custom_call_target="tpu_custom_call" | custom-call | tf_op jit(solution)/shard_map/pallas_call | solution.py:1062
  22.0 1.4 %shard_map.141 = (bf16[16,4,512]{2,1,0:T(4,128)(2,1)}, f32[4,8,128,128]{3,2,1,0:T(8,128)}) custom-call(f32[4,8,128,128]{3,2,1,0:T(8,128)S(1)} %get-tuple-element.6.tk_v, f32[2,64,512]{2,1,0:T(8,128)S(1)} %get-tuple-element.7.acc_v, bf16[2,64,256]{2,1,0:T(8,128)(2,1)S(1)} %get-tuple-element.8.last_v, bf16[2,256,512]{2,1,0:T(8,128)(2,1)S(1)} %get-tuple-element.9.wl_v), custom_call_target="tpu_custom_call" | custom-call | tf_op jit(solution)/shard_map/pallas_call | solution.py:1087

commit v3 on v2

--- a/solution.py
+++ b/solution.py
@@ -27,17 +27,13 @@
     "2 to 3": (2, 3, 3, 1),
     "2 to 0": (2, 0, 0, 1),
     "2 to 1": (2, 1, 1, 1),
-    "3 for 0": (3, 2, 0, 3),
+    "3 for 1": (3, 2, 1, 3),
     "3 to 1": (3, 1, 1, 2),
     "3 to 2": (3, 2, 2, 1),
+    "3 to 0": (3, 0, 0, 2),
 }
 OWN = 3
-FIRST = {0: ("0 for 3",), 1: ("1 to 0",), 2: ("2 to 1", "2 to 3"), 3: ("3 for 0",)}
-THEN = {0: ("0 for 2", "0 to 1"), 3: ("3 to 1", "3 to 2")}
-ONWARD = {
-    1: (("0 for 3", "1 to 3"), ("0 for 2", "1 to 2")),
-    2: (("3 for 0", "2 to 0"), None),
-}
+DIRECT = 1
 PEERS = ((3, 2, 1), (3, 2, 0), (0, 1, 3), (0, 1, 2))
 
 
@@ -643,21 +639,25 @@
     pl.semaphore_wait(barrier, jnp.where(at_end, tp, tp + 1))
     ssq_copy(0, 0, partner).start()
 
+    def go(to):
+        pl.semaphore_signal(
+            go_sem, inc=1, device_id={"kv": to}, device_id_type=pl.DeviceIdType.MESH
+        )
+
     @pl.when(inside)
     def _():
-        pl.semaphore_signal(
-            go_sem, inc=1, device_id={"kv": across}, device_id_type=pl.DeviceIdType.MESH
-        )
-
-    @pl.when(me == 2)
-    def _():
-        pl.semaphore_signal(
-            go_sem, inc=1, device_id={"kv": 3}, device_id_type=pl.DeviceIdType.MESH
-        )
-
-    @pl.when(me != 1)
-    def _():
-        recv_v[:, OWN - 1] = jnp.zeros_like(recv_v[:, OWN - 1])
+        go(across)
+
+    direct = chunks - DIRECT
+
+    def terms_of(c):
+        return (me == 0) if c < direct else (me < 2)
+
+    for c in range(chunks):
+
+        @pl.when(jnp.logical_not(terms_of(c)))
+        def _():
+            recv_v[c, OWN - 1] = jnp.zeros_like(recv_v[c, OWN - 1])
 
     place = lax.broadcasted_iota(jnp.int32, (own_rows, 1), 0)
     prop = lax.rem(place, props)
@@ -710,47 +710,73 @@
         prod_v[c] = product
         send_v[c] = product.astype(BF16)
 
-        for device, names in FIRST.items():
-
-            @pl.when(me == device)
-            def _():
-                for name in names:
-                    message(c, name).start()
-
-    for device, names in THEN.items():
-
-        @pl.when(me == device)
-        def _():
-            if device == 3:
+        @pl.when(me == 0)
+        def _():
+            message(c, "0 for 3").start()
+
+        @pl.when(me == 1)
+        def _():
+            message(c, "1 to 0").start()
+
+        @pl.when(me == 2)
+        def _():
+            message(c, "2 to 3").start()
+            if c == 0:
                 pl.semaphore_wait(go_sem, 1)
-            for name in names:
-                for c in range(chunks):
-                    message(c, name).start()
+                go(3)
+            message(c, "2 to 0").start()
+            if c >= direct:
+                message(c, "2 to 1").start()
+
+        @pl.when(me == 3)
+        def _():
+            if c == direct:
+                pl.semaphore_wait(go_sem, 1)
+            message(c, "3 to 1" if c >= direct else "3 for 1").start()
+
+    @pl.when(me == 0)
+    def _():
+        for name in ("0 for 2", "0 to 1"):
+            for c in range(chunks):
+                message(c, name).start()
+
+    @pl.when(me == 3)
+    def _():
+        for name in ("3 to 2", "3 to 0"):
+            for c in range(chunks):
+                message(c, name).start()
 
     terms = old_terms()
     ssq_copy(0, 0, partner).wait_recv()
 
+    @pl.when(me == 1)
+    def _():
+        pl.semaphore_wait(go_sem, 1)
+
     @pl.when(inside)
     def _():
-        pl.semaphore_wait(go_sem, 1)
         ssq_s[1] = ssq_v[...] + ssq_r[0]
         ssq_copy(1, 1, across).start()
         ssq_s[2] = ssq_v[...] + ssq_r[0]
         ssq_copy(2, 1, beyond).start()
 
     for c in range(chunks):
-        for device, steps in ONWARD.items():
-
-            @pl.when(me == device)
+        @pl.when(me == 1)
+        def _():
+            pass_on(c, "0 for 3", "1 to 3")
+
+        if c < direct:
+
+            @pl.when(me == 2)
             def _():
-                pass_on(c, *steps[0])
+                pass_on(c, "3 for 1", "2 to 1")
 
         take(c, *terms)
 
     @pl.when(me == 1)
     def _():
         for c in range(chunks):
-            pass_on(c, *ONWARD[1][1])
+            pass_on(c, "0 for 2", "1 to 2")
 
     for o in range(1, tp):
         cols = pl.ds(pl.multiple_of(tp_peers[o - 1] * half, half), half)
@@ -804,11 +830,11 @@
         )
 
     def recur(c):
-        @pl.when(me == 1)
+        @pl.when(terms_of(c))
         def _():
             held(recv_v.at[c, :OWN], rs_rsem.at[c, 0])
 
-        @pl.when(me != 1)
+        @pl.when(jnp.logical_not(terms_of(c)))
         def _():
             held(recv_v.at[c, : OWN - 1], rs_rsem.at[c, 0])
 

time: 23.5 us -> 23.4 us (level)
  no operation moved by 1% of the time
where the time goes in v3:
time: 23.4 us; the launch traced here: 23.3 us
  Pallas kernels  22.6 us (97%)
  between operations  0.64 us (3%)
    pallas_call x1, Pallas kernels, per_device(): pl.pallas_call(body, out_shape=outs, in_specs=[pl.BlockSpec(memory_space=...  21.3 us
    pallas_call x1, Pallas kernels, per_device(): pl.pallas_call(last, out_shape=(jax.ShapeDtypeStruct((seqs, props, half),...  1.36 us

profile of v3, /device:TPU:1, one launch (start us, length us, event | category | flops | bytes accessed | tf_op | source)
XLA Modules:
  0.0 23.3 jit_solution(8892738711228906631)
XLA Ops:
  0.6 21.3 %shard_map.140 = (f32[4,8,128,128]{3,2,1,0:T(8,128)S(1)}, f32[2,64,512]{2,1,0:T(8,128)S(1)}, bf16[2,64,256]{2,1,0:T(8,128)(2,1)S(1)}, bf16[2,256,512]{2,1,0:T(8,128)(2,1)S(1)}) custom-call(bf16[16,4,1024]{2,1,0:T(4,128)(2,1)} %tokens.1, bf16[1024,1024]{1,0:T(8,128)(2,1)} %w_query.1, bf16[1024,1024]{1,0:T(8,128)(2,1)} %w_forget.1, ...), custom_call_target="tpu_custom_call" | custom-call | tf_op jit(solution)/shard_map/pallas_call | solution.py:1088
  21.9 1.4 %shard_map.141 = (bf16[16,4,512]{2,1,0:T(4,128)(2,1)}, f32[4,8,128,128]{3,2,1,0:T(8,128)}) custom-call(f32[4,8,128,128]{3,2,1,0:T(8,128)S(1)} %get-tuple-element.6.tk_v, f32[2,64,512]{2,1,0:T(8,128)S(1)} %get-tuple-element.7.acc_v, bf16[2,64,256]{2,1,0:T(8,128)(2,1)S(1)} %get-tuple-element.8.last_v, bf16[2,256,512]{2,1,0:T(8,128)(2,1)S(1)} %get-tuple-element.9.wl_v), custom_call_target="tpu_custom_call" | custom-call | tf_op jit(solution)/shard_map/pallas_call | solution.py:1113

commit v4 on v3

--- a/solution.py
+++ b/solution.py
@@ -34,7 +34,7 @@
 }
 OWN = 3
 DIRECT = 1
-PEERS = ((3, 2, 1), (3, 2, 0), (0, 1, 3), (0, 1, 2))
+PEERS = ((3, 2, 1), (3, 2, 0), (0, 3, 1), (0, 1, 2))
 
 
 def kernel_any(
@@ -592,20 +592,15 @@
             device_id_type=pl.DeviceIdType.MESH,
         )
 
-    tok_c.wait()
     gain_c.wait()
     load_w(1)
+    tok_c.wait()
     load_w(2)
     for s in range(seqs):
         rows_v[pl.ds(s * props, props), :] = tok_v[s].astype(F32)
     x = rows_v[...]
     my_gain = gain_v[:, pl.ds(pl.multiple_of(me * feat, feat), feat)]
     scaled_v[...] = (x * my_gain).astype(BF16)
-    squared = jnp.sum(x * x, axis=1, keepdims=True)
-    on_row = lax.broadcasted_iota(jnp.int32, (rows, HEAD), 0)
-    on_lane = lax.broadcasted_iota(jnp.int32, (rows, HEAD), 1)
-    along = jnp.sum(jnp.where(on_row == on_lane, squared, 0.0), axis=0, keepdims=True)
-    ssq_v[...] = jnp.broadcast_to(along, ssq_v.shape)
 
     def rows_of(device):
         return pl.ds(pl.multiple_of(device * own_rows, own_rows), own_rows)
@@ -631,14 +626,11 @@
     def ssq_copy(i, slot, to):
         return remote(ssq_s.at[i], ssq_r.at[slot], ssq_ssem.at[i], ssq_rsem.at[slot], "kv", to)
 
-    ssq_s[0] = ssq_v[...]
     partner = me + 1 - 2 * lax.rem(me, 2)
     across = jnp.where(me == 1, 2, 1)
     beyond = jnp.where(me == 1, 3, 0)
     inside = jnp.logical_not(at_end)
     pl.semaphore_wait(barrier, jnp.where(at_end, tp, tp + 1))
-    ssq_copy(0, 0, partner).start()
-
     def go(to):
         pl.semaphore_signal(
             go_sem, inc=1, device_id={"kv": to}, device_id_type=pl.DeviceIdType.MESH
@@ -653,11 +645,6 @@
     def terms_of(c):
         return (me == 0) if c < direct else (me < 2)
 
-    for c in range(chunks):
-
-        @pl.when(jnp.logical_not(terms_of(c)))
-        def _():
-            recv_v[c, OWN - 1] = jnp.zeros_like(recv_v[c, OWN - 1])
 
     place = lax.broadcasted_iota(jnp.int32, (own_rows, 1), 0)
     prop = lax.rem(place, props)
@@ -734,6 +721,16 @@
                 pl.semaphore_wait(go_sem, 1)
             message(c, "3 to 1" if c >= direct else "3 for 1").start()
 
+        if c == 0:
+            x = rows_v[...]
+            squared = jnp.sum(x * x, axis=1, keepdims=True)
+            on_row = lax.broadcasted_iota(jnp.int32, (rows, HEAD), 0)
+            on_lane = lax.broadcasted_iota(jnp.int32, (rows, HEAD), 1)
+            along = jnp.sum(jnp.where(on_row == on_lane, squared, 0.0), axis=0, keepdims=True)
+            ssq_v[...] = along
+            ssq_s[0] = along
+            ssq_copy(0, 0, partner).start()
+
     @pl.when(me == 0)
     def _():
         for name in ("0 for 2", "0 to 1"):
@@ -745,6 +742,12 @@
         for name in ("3 to 2", "3 to 0"):
             for c in range(chunks):
                 message(c, name).start()
+
+    for c in range(chunks):
+
+        @pl.when(jnp.logical_not(terms_of(c)))
+        def _():
+            recv_v[c, OWN - 1] = jnp.zeros_like(recv_v[c, OWN - 1])
 
     terms = old_terms()
     ssq_copy(0, 0, partner).wait_recv()
@@ -828,6 +831,13 @@
             gath_v.at[0, c], gath_v.at[tp - o, c], fw_ssem.at[c, o - 1],
             fw_rsem.at[c, tp - o - 1], "tp", tp_peers[o - 1],
         )
+
+    def send_heads(c, o):
+        if o < kv - 1:
+            head_copy(c, o).start()
+        if c >= crossed:
+            for away in range(1, tp):
+                cross_copy(c, away, o).start()
 
     def recur(c):
         @pl.when(terms_of(c))
@@ -883,11 +893,12 @@
             normed = r * lax.rsqrt(jnp.mean(r * r, axis=1, keepdims=True) + EPSILON)
             outs.append((normed * gate[:, cols]).astype(BF16))
         heads_of(c, 0)[mine_rows, :] = jnp.concatenate(outs, axis=1)
-        for o in range(kv - 1):
-            head_copy(c, o).start()
-        if c >= crossed:
-            for copy in cross_copies(c):
-                copy.start()
+        for o in (0, 1, kv - 1):
+            send_heads(c, o)
+
+        @pl.when(me != 2)
+        def _():
+            send_heads(c, 2)
 
     def gathered(c):
         held(heads_of(c, 0).at[: (kv - 1) * own_rows], ag_rsem.at[c])
@@ -907,6 +918,12 @@
 
     for c in range(chunks):
         recur(c)
+
+    @pl.when(me == 2)
+    def _():
+        for c in range(chunks):
+            send_heads(c, 2)
+
     out_held(wo_sem)
     for o in range(1, tp):
         out_held(wo_rsem.at[o - 1])

time: 23.4 us -> 22.9 us (0.979)
  Pallas kernels: 22.6 us -> 21.9 us
    pallas_call x1, Pallas kernels: 21.3 us -> 20.6 us  [per_device(): pl.pallas_call(body, out_shape=outs, in_specs=[pl.BlockSpec(memory_space=...]
where the time goes in v4:
time: 22.9 us; the launch traced here: 22.6 us
  Pallas kernels  21.9 us (96%)
  between operations  0.64 us (3%)
    pallas_call x1, Pallas kernels, per_device(): pl.pallas_call(body, out_shape=outs, in_specs=[pl.BlockSpec(memory_space=...  20.6 us
    pallas_call x1, Pallas kernels, per_device(): pl.pallas_call(last, out_shape=(jax.ShapeDtypeStruct((seqs, props, half),...  1.36 us

profile of v4, /device:TPU:1, one launch (start us, length us, event | category | flops | bytes accessed | tf_op | source)
XLA Modules:
  0.0 22.6 jit_solution(17363564120715976403)
XLA Ops:
  0.6 20.6 %shard_map.140 = (f32[4,8,128,128]{3,2,1,0:T(8,128)S(1)}, f32[2,64,512]{2,1,0:T(8,128)S(1)}, bf16[2,64,256]{2,1,0:T(8,128)(2,1)S(1)}, bf16[2,256,512]{2,1,0:T(8,128)(2,1)S(1)}) custom-call(bf16[16,4,1024]{2,1,0:T(4,128)(2,1)} %tokens.1, bf16[1024,1024]{1,0:T(8,128)(2,1)} %w_query.1, bf16[1024,1024]{1,0:T(8,128)(2,1)} %w_forget.1, ...), custom_call_target="tpu_custom_call" | custom-call | tf_op jit(solution)/shard_map/pallas_call | solution.py:1105
  21.2 1.4 %shard_map.141 = (bf16[16,4,512]{2,1,0:T(4,128)(2,1)}, f32[4,8,128,128]{3,2,1,0:T(8,128)}) custom-call(f32[4,8,128,128]{3,2,1,0:T(8,128)S(1)} %get-tuple-element.6.tk_v, f32[2,64,512]{2,1,0:T(8,128)S(1)} %get-tuple-element.7.acc_v, bf16[2,64,256]{2,1,0:T(8,128)(2,1)S(1)} %get-tuple-element.8.last_v, bf16[2,256,512]{2,1,0:T(8,128)(2,1)S(1)} %get-tuple-element.9.wl_v), custom_call_target="tpu_custom_call" | custom-call | tf_op jit(solution)/shard_map/pallas_call | solution.py:1130

commit v5 on v4

--- a/solution.py
+++ b/solution.py
@@ -900,6 +900,12 @@
         def _():
             send_heads(c, 2)
 
+        if c >= 2:
+
+            @pl.when(me == 2)
+            def _():
+                send_heads(c - 2, 2)
+
     def gathered(c):
         held(heads_of(c, 0).at[: (kv - 1) * own_rows], ag_rsem.at[c])
 
@@ -921,7 +927,7 @@
 
     @pl.when(me == 2)
     def _():
-        for c in range(chunks):
+        for c in range(chunks - 2, chunks):
             send_heads(c, 2)
 
     out_held(wo_sem)
@@ -934,11 +940,16 @@
                 forward(c, o).start()
         if c < chunks - 1:
             product_of(c, 0)
-        if c > 0:
-            from_tp(c - 1)
+        if c == chunks - 2:
+            for early in range(chunks - 2):
+                from_tp(early)
+                for o in range(1, tp):
+                    product_of(early, o)
+    for c in range(chunks - 2, chunks):
+        from_tp(c)
+        if c < chunks - 1:
             for o in range(1, tp):
-                product_of(c - 1, o)
-    from_tp(chunks - 1)
+                product_of(c, o)
 
     held(send_v.at[:, : (kv - 1) * own_rows], rs_ssem)
     ssq_copy(0, 0, partner).wait_send()

time: 22.9 us -> 22.7 us (level)
  no operation moved by 1% of the time
where the time goes in v5:
time: 22.7 us; the launch traced here: 22.6 us
  Pallas kernels  21.9 us (96%)
  between operations  0.64 us (3%)
    pallas_call x1, Pallas kernels, per_device(): pl.pallas_call(body, out_shape=outs, in_specs=[pl.BlockSpec(memory_space=...  20.6 us
    pallas_call x1, Pallas kernels, per_device(): pl.pallas_call(last, out_shape=(jax.ShapeDtypeStruct((seqs, props, half),...  1.36 us

profile of v5, /device:TPU:1, one launch (start us, length us, event | category | flops | bytes accessed | tf_op | source)
XLA Modules:
  0.0 22.6 jit_solution(8846720417065948123)
XLA Ops:
  0.6 20.6 %shard_map.140 = (f32[4,8,128,128]{3,2,1,0:T(8,128)S(1)}, f32[2,64,512]{2,1,0:T(8,128)S(1)}, bf16[2,64,256]{2,1,0:T(8,128)(2,1)S(1)}, bf16[2,256,512]{2,1,0:T(8,128)(2,1)S(1)}) custom-call(bf16[16,4,1024]{2,1,0:T(4,128)(2,1)} %tokens.1, bf16[1024,1024]{1,0:T(8,128)(2,1)} %w_query.1, bf16[1024,1024]{1,0:T(8,128)(2,1)} %w_forget.1, ...), custom_call_target="tpu_custom_call" | custom-call | tf_op jit(solution)/shard_map/pallas_call | solution.py:1116
  21.2 1.4 %shard_map.141 = (bf16[16,4,512]{2,1,0:T(4,128)(2,1)}, f32[4,8,128,128]{3,2,1,0:T(8,128)}) custom-call(f32[4,8,128,128]{3,2,1,0:T(8,128)S(1)} %get-tuple-element.6.tk_v, f32[2,64,512]{2,1,0:T(8,128)S(1)} %get-tuple-element.7.acc_v, bf16[2,64,256]{2,1,0:T(8,128)(2,1)S(1)} %get-tuple-element.8.last_v, bf16[2,256,512]{2,1,0:T(8,128)(2,1)S(1)} %get-tuple-element.9.wl_v), custom_call_target="tpu_custom_call" | custom-call | tf_op jit(solution)/shard_map/pallas_call | solution.py:1141

commit v6 on v5

--- a/solution.py
+++ b/solution.py
@@ -34,7 +34,7 @@
 }
 OWN = 3
 DIRECT = 1
-PEERS = ((3, 2, 1), (3, 2, 0), (0, 3, 1), (0, 1, 2))
+PEERS = ((3, 2, 1), (0, 3, 2), (0, 3, 1), (0, 1, 2))
 
 
 def kernel_any(
@@ -828,7 +828,7 @@
 
     def forward(c, o):
         return remote(
-            gath_v.at[0, c], gath_v.at[tp - o, c], fw_ssem.at[c, o - 1],
+            gath_v.at[0, c], gath_v.at[tp - o, c], fw_ssem.at[o - 1],
             fw_rsem.at[c, tp - o - 1], "tp", tp_peers[o - 1],
         )
 
@@ -963,9 +963,8 @@
     held(w_v.at[0, : blocks * own_rows // 4], ag_ssem)
     for o in range(1, tp):
         out_held(wo_ssem.at[o - 1])
-    for c in range(crossed):
-        for o in range(1, tp):
-            forward(c, o).wait_send()
+    for o in range(1, tp):
+        held(gath_v.at[0, :crossed], fw_ssem.at[o - 1])
 
 
 def finish_line(tk_v, acc_v, last_v, wl_v, mixed, taken, mix_v, sem):
@@ -1073,7 +1072,7 @@
             dma,
             dma((chunks,)),
             dma((CROSS, tp - 1)),
-            dma((chunks - CROSS, tp - 1)),
+            dma((tp - 1,)),
             dma((chunks - CROSS, tp - 1)),
             dma((tp - 1,)),
             dma((tp - 1,)),

time: 22.7 us -> 22.7 us (level)
  no operation moved by 1% of the time
where the time goes in v6:
time: 22.7 us; the launch traced here: 22.5 us
  Pallas kernels  21.9 us (96%)
  between operations  0.64 us (3%)
    pallas_call x1, Pallas kernels, per_device(): pl.pallas_call(body, out_shape=outs, in_specs=[pl.BlockSpec(memory_space=...  20.5 us
    pallas_call x1, Pallas kernels, per_device(): pl.pallas_call(last, out_shape=(jax.ShapeDtypeStruct((seqs, props, half),...  1.36 us

profile of v6, /device:TPU:1, one launch (start us, length us, event | category | flops | bytes accessed | tf_op | source)
XLA Modules:
  0.0 22.5 jit_solution(824921596570417494)
XLA Ops:
  0.6 20.5 %shard_map.140 = (f32[4,8,128,128]{3,2,1,0:T(8,128)S(1)}, f32[2,64,512]{2,1,0:T(8,128)S(1)}, bf16[2,64,256]{2,1,0:T(8,128)(2,1)S(1)}, bf16[2,256,512]{2,1,0:T(8,128)(2,1)S(1)}) custom-call(bf16[16,4,1024]{2,1,0:T(4,128)(2,1)} %tokens.1, bf16[1024,1024]{1,0:T(8,128)(2,1)} %w_query.1, bf16[1024,1024]{1,0:T(8,128)(2,1)} %w_forget.1, ...), custom_call_target="tpu_custom_call" | custom-call | tf_op jit(solution)/shard_map/pallas_call | solution.py:1115
  21.2 1.4 %shard_map.141 = (bf16[16,4,512]{2,1,0:T(4,128)(2,1)}, f32[4,8,128,128]{3,2,1,0:T(8,128)}) custom-call(f32[4,8,128,128]{3,2,1,0:T(8,128)S(1)} %get-tuple-element.6.tk_v, f32[2,64,512]{2,1,0:T(8,128)S(1)} %get-tuple-element.7.acc_v, bf16[2,64,256]{2,1,0:T(8,128)(2,1)S(1)} %get-tuple-element.8.last_v, bf16[2,256,512]{2,1,0:T(8,128)(2,1)S(1)} %get-tuple-element.9.wl_v), custom_call_target="tpu_custom_call" | custom-call | tf_op jit(solution)/shard_map/pallas_call | solution.py:1140
